TPU v7x, 32 devices: a whole 2x2x4 slice. The times are simulated.
32 devices in a mesh: sp: 8 (over z, core), tp: 4 (over y, x).
Axes of the slice: x: 2, y: 2, z: 4, core: 2. Of those that a mesh axis runs over, the one named last changes fastest.
Arguments:
- moe_input: bfloat16 [2560, 2048], P('sp', 'tp'), may hold values from -6 to 6
- out_cotangent: bfloat16 [2560, 2048], P('sp', 'tp'), may hold values from -0.59765625 to 0.59765625
- routes: int32 [2560, 2], P('sp'), may hold values from 0 to 7, all different within a row; in each aligned block of 320 rows (0 to 319, 320 to 639, ...) at most 120 rows name the same one
- route_weight: float32 [2560, 2], P('sp'), may hold values from 0.1 to 0.9
- gate_weight: bfloat16 [8, 1024, 2048], P('sp', 'tp'), may hold values from -0.125 to 0.125
- up_weight: bfloat16 [8, 1024, 2048], P('sp', 'tp'), may hold values from -0.125 to 0.125
- down_weight: bfloat16 [8, 1024, 2048], P('sp', 'tp'), may hold values from -0.1875 to 0.1875
- glu_value: bfloat16 [2560, 1024], P('sp', 'tp'), may hold values from -6 to 6
- glu_gate: bfloat16 [2560, 1024], P('sp', 'tp'), may hold values from -8 to 8
- conv_result: bfloat16 [2560, 1024], P('sp', 'tp'), may hold values from -12 to 12
- conv_taps: float32 [31, 1024], P(None, 'tp'), may hold values from -1 to 1
- norm_gain: float32 [1024], P('tp'), may hold values from 0.1 to 1.9
- proj_weight: bfloat16 [1024, 2048], P('tp'), may hold values from -0.1875 to 0.1875
Outputs:
- grad_gate: float32 [8, 1024, 2048], P('sp', 'tp')
- grad_up: float32 [8, 1024, 2048], P('sp', 'tp')
- grad_down: float32 [8, 1024, 2048], P('sp', 'tp')
- grad_proj: float32 [2048, 1024], P('sp', 'tp')
- grad_value: bfloat16 [2560, 1024], P('sp', 'tp')
- grad_glu_gate: bfloat16 [2560, 1024], P('sp', 'tp')
Inputs may be any that keep to these rules, and one draw needn't show every extreme that they name: `routes`: each row names two different experts. In the aligned blocks of 320 rows (the rows of one index of sp) no expert is named by more than 120 rows, and that bound is reached.
All inputs are finite; a program needn't handle non-finite values.
Results may differ from a plain program's by a relative error of at most 0.025.
Values may be sent and summed in bfloat16 or wider, within the bound.
A program may use at most 64 MiB of HBM per device.

v0:
```python
import functools

import jax
import jax.numpy as jnp
from jax import lax
from jax.experimental import pallas as pl
from jax.experimental.pallas import tpu as pltpu
from jax.sharding import PartitionSpec as P

C = 1024


NORM_EPS = 0.25


MESH = pl.DeviceIdType.MESH


def from_behind(value, axis, steps):
    count = lax.axis_size(axis)
    leading, last = (max(0, -steps), min(count, count - steps))
    return lax.ppermute(value, axis, [(source, source + steps) for source in range(leading, last)])


def pair_places(route_ids, experts, capacity):
    flat_ids = route_ids.reshape(-1)
    onehot = (flat_ids[:, None] == jnp.arange(experts, dtype=jnp.int32)[None, :]).astype(jnp.int32)
    earlier = jnp.cumsum(onehot, axis=0) - onehot
    slot_rank = jnp.sum(earlier * onehot, axis=1)
    return flat_ids * capacity + slot_rank


def place_rows(values, target, experts, capacity):
    empty_rows = jnp.zeros((experts * capacity, values.shape[1]), values.dtype)
    return empty_rows.at[target].set(values).reshape(experts, capacity, values.shape[1])


def flip(index, mask):
    result, bit = index, 1
    while bit <= mask:
        if mask & bit:
            result = result + bit * (1 - 2 * ((index // bit) % 2))
        bit *= 2
    return result


def greet(sp, tp, n_sp, n_tp):
    barrier = pltpu.get_barrier_semaphore()
    for mask in range(1, n_sp):
        pl.semaphore_signal(barrier, inc=1, device_id=(flip(sp, mask), tp), device_id_type=MESH)
    for mask in range(1, n_tp):
        pl.semaphore_signal(barrier, inc=1, device_id=(sp, flip(tp, mask)), device_id_type=MESH)
    pl.semaphore_wait(barrier, n_sp + n_tp - 2)


def columns(index, width):
    return pl.ds(pl.multiple_of(index * width, width), width)


def dispatch_kernel(
    n_sp, rows_ref, cot_ref, stats_ref, full_rows, full_cot, all_stats,
    local_sem, stat_send, stat_recv, sp_send, sp_recv, tp_send, tp_recv,
):
    n_tp = 4
    sp, tp = lax.axis_index("sp"), lax.axis_index("tp")
    width = rows_ref.shape[2]
    arrays = ((rows_ref, full_rows), (cot_ref, full_cot))
    greet(sp, tp, n_sp, n_tp)
    started = []

    def from_sp(which, step):
        source, target = arrays[which]
        peer = flip(sp, step)
        return pltpu.make_async_remote_copy(
            src_ref=source.at[peer],
            dst_ref=target.at[sp, :, columns(tp, width)],
            send_sem=sp_send.at[which, step],
            recv_sem=sp_recv.at[which, step],
            device_id=(peer, tp),
            device_id_type=MESH,
        )

    def along_tp(which, step, origin, hop, slot):
        target = arrays[which][1]
        block = target.at[flip(sp, step), :, columns(flip(tp, origin), width)]
        return pltpu.make_async_remote_copy(
            src_ref=block,
            dst_ref=block,
            send_sem=tp_send.at[which, step, slot],
            recv_sem=tp_recv.at[which, step, slot],
            device_id=(sp, flip(tp, hop)),
            device_id_type=MESH,
        )

    own = []
    for which in range(2):
        source, target = arrays[which]
        copy = pltpu.make_async_copy(
            source.at[sp], target.at[sp, :, columns(tp, width)], local_sem.at[which]
        )
        copy.start()
        own.append(copy)
        for step in range(1, n_sp):
            copy = from_sp(which, step)
            copy.start()
            started.append(copy)
    stat_copies = []
    for mask in range(1, n_tp):
        copy = pltpu.make_async_remote_copy(
            src_ref=stats_ref,
            dst_ref=all_stats.at[mask],
            send_sem=stat_send.at[mask],
            recv_sem=stat_recv.at[mask],
            device_id=(sp, flip(tp, mask)),
            device_id_type=MESH,
        )
        copy.start()
        stat_copies.append(copy)
    all_stats[0] = stats_ref[...]

    lag = 1
    work = [(which, step) for which in range(2) for step in range(n_sp)]
    hops = {}
    for turn in range(len(work) + lag):
        if turn < len(work):
            which, step = work[turn]
            if step == 0:
                own[which].wait()
            else:
                from_sp(which, step).wait_recv()
            first, second = (1, 2) if step % 2 == 0 else (2, 1)
            near = along_tp(which, step, 0, first, 0)
            near.start()
            far = along_tp(which, step, 0, second, 1)
            far.start()
            hops[turn] = (near, far)
        if turn >= lag:
            which, step = work[turn - lag]
            first, second = (1, 2) if step % 2 == 0 else (2, 1)
            near, far = hops[turn - lag]
            near.wait_recv()
            onward = along_tp(which, step, first, second, 2)
            onward.start()
            hops[turn - lag] = (near, far, onward)
    for turn in range(len(work)):
        near, far, onward = hops[turn]
        far.wait_recv()
        onward.wait_recv()
        near.wait_send()
        far.wait_send()
        onward.wait_send()
    for copy in started:
        copy.wait_send()
    for copy in stat_copies:
        copy.wait()


def dispatch(sent_rows, sent_cot, stats, n_sp):
    experts, capacity, width = sent_rows.shape
    full = jax.ShapeDtypeStruct((experts, capacity, 4 * width), sent_rows.dtype)
    vmem = pl.BlockSpec(memory_space=pltpu.VMEM)
    dma = pltpu.SemaphoreType.DMA
    return pl.pallas_call(
        functools.partial(dispatch_kernel, n_sp),
        out_shape=(full, full, jax.ShapeDtypeStruct((4,) + stats.shape, stats.dtype)),
        in_specs=[vmem] * 3,
        out_specs=(vmem,) * 3,
        scratch_shapes=[
            dma((2,)), dma((4,)), dma((4,)),
            dma((2, n_sp)), dma((2, n_sp)), dma((2, n_sp, 3)), dma((2, n_sp, 3)),
        ],
        compiler_params=pltpu.CompilerParams(collective_id=0, has_side_effects=True),
    )(sent_rows, sent_cot, stats)


def return_kernel(
    n_sp, partial_ref, out_ref, landed, passing, finished, tp_send, tp_recv, sp_send, sp_recv
):
    n_tp = 4
    sp, tp = lax.axis_index("sp"), lax.axis_index("tp")
    width = out_ref.shape[2]
    greet(sp, tp, n_sp, n_tp)

    def order(turn):
        return (1, 2) if turn % 2 == 0 else (2, 1)

    def step_of(turn):
        return n_sp - 1 - turn

    def piece(turn, mask):
        return partial_ref.at[flip(sp, step_of(turn)), :, columns(flip(tp, mask), width)]

    def along_tp(turn, source, hop, slot):
        return pltpu.make_async_remote_copy(
            src_ref=source,
            dst_ref=landed.at[turn, slot],
            send_sem=tp_send.at[turn, slot],
            recv_sem=tp_recv.at[turn, slot],
            device_id=(sp, flip(tp, hop)),
            device_id_type=MESH,
        )

    def read(turn, mask):
        return piece(turn, mask)[...].astype(jnp.float32)

    crossing, direct, summed, home = {}, {}, {}, {}
    for turn in range(n_sp):
        first, second = order(turn)
        crossing[turn] = along_tp(turn, piece(turn, first + second), first, 1)
        crossing[turn].start()
        direct[turn] = along_tp(turn, piece(turn, first), first, 0)
        direct[turn].start()
    for turn in range(n_sp + 1):
        if turn < n_sp:
            first, second = order(turn)
            crossing[turn].wait_recv()
            passing[turn] = (
                read(turn, second) + landed[turn, 1].astype(jnp.float32)
            ).astype(passing.dtype)
            summed[turn] = along_tp(turn, passing.at[turn], second, 2)
            summed[turn].start()
        if turn >= 1:
            last = turn - 1
            direct[last].wait_recv()
            summed[last].wait_recv()
            total = (
                read(last, 0)
                + landed[last, 0].astype(jnp.float32)
                + landed[last, 2].astype(jnp.float32)
            ).astype(finished.dtype)
            step = step_of(last)
            if step == 0:
                out_ref[sp] = total
            else:
                finished[step] = total
                home[step] = pltpu.make_async_remote_copy(
                    src_ref=finished.at[step],
                    dst_ref=out_ref.at[sp],
                    send_sem=sp_send.at[step],
                    recv_sem=sp_recv.at[step],
                    device_id=(flip(sp, step), tp),
                    device_id_type=MESH,
                )
                home[step].start()
    for turn in range(n_sp):
        crossing[turn].wait_send()
        direct[turn].wait_send()
        summed[turn].wait_send()
    for step in range(1, n_sp):
        home[step].wait()


def send_home(partial, n_sp):
    experts, capacity, full = partial.shape
    width = full // 4
    vmem = pl.BlockSpec(memory_space=pltpu.VMEM)
    dma = pltpu.SemaphoreType.DMA
    return pl.pallas_call(
        functools.partial(return_kernel, n_sp),
        out_shape=jax.ShapeDtypeStruct((experts, capacity, width), partial.dtype),
        in_specs=[vmem],
        out_specs=vmem,
        scratch_shapes=[
            pltpu.VMEM((n_sp, 3, capacity, width), partial.dtype),
            pltpu.VMEM((n_sp, capacity, width), partial.dtype),
            pltpu.VMEM((n_sp, capacity, width), partial.dtype),
            dma((n_sp, 3)), dma((n_sp, 3)), dma((n_sp,)), dma((n_sp,)),
        ],
        compiler_params=pltpu.CompilerParams(collective_id=1, has_side_effects=True),
    )(partial)


def contract_rows(left, right):
    return lax.dot_general(
        left, right, (((0,), (0,)), ((), ())), preferred_element_type=jnp.float32
    )


def contract_cols(left, right):
    return lax.dot_general(
        left, right, (((1,), (1,)), ((), ())), preferred_element_type=jnp.float32
    )


def expert_backward(token_rows, cot_rows, gate_matrix, up_matrix, down_matrix):
    gate_pre = contract_cols(token_rows, gate_matrix)
    up_pre = contract_cols(token_rows, up_matrix)
    gate_sigmoid = jax.nn.sigmoid(gate_pre)
    activation = gate_pre * gate_sigmoid
    hidden = (activation * up_pre).astype(jnp.bfloat16)
    grad_down = contract_rows(hidden, cot_rows)
    hidden_cot = contract_cols(cot_rows, down_matrix)
    up_cot = (hidden_cot * activation).astype(jnp.bfloat16)
    gate_cot = (
        hidden_cot * up_pre * gate_sigmoid * (1.0 + gate_pre * (1.0 - gate_sigmoid))
    ).astype(jnp.bfloat16)
    grad_gate = contract_rows(gate_cot, token_rows)
    grad_up = contract_rows(up_cot, token_rows)
    partial_value = jnp.dot(gate_cot, gate_matrix, preferred_element_type=jnp.float32) + jnp.dot(
        up_cot, up_matrix, preferred_element_type=jnp.float32
    )
    return (
        grad_gate[None],
        grad_up[None],
        grad_down[None],
        partial_value.astype(jnp.bfloat16)[None],
    )


def body(
    moe_input,
    out_cotangent,
    routes,
    route_weight,
    gate_weight,
    up_weight,
    down_weight,
    glu_value,
    glu_gate,
    conv_result,
    conv_taps,
    norm_gain,
    proj_weight,
):
    sp_count = lax.axis_size("sp")
    token_count = moe_input.shape[0]
    experts = sp_count * gate_weight.shape[0]
    capacity = 3 * token_count // experts
    target = pair_places(routes, experts, capacity).reshape(token_count, 2)
    slots = jnp.arange(experts * capacity, dtype=jnp.int32)[:, None]
    first_here, second_here = slots == target[None, :, 0], slots == target[None, :, 1]
    pick = (first_here | second_here).astype(jnp.bfloat16)
    slot_weight = jnp.sum(
        jnp.where(first_here, route_weight[None, :, 0], 0.0)
        + jnp.where(second_here, route_weight[None, :, 1], 0.0),
        axis=1,
    )
    shape = (experts, capacity, moe_input.shape[1])
    sent_rows = (
        jnp.dot(pick, moe_input, preferred_element_type=jnp.float32)
        .astype(jnp.bfloat16)
        .reshape(shape)
    )
    sent_cot = (
        (slot_weight[:, None] * jnp.dot(pick, out_cotangent, preferred_element_type=jnp.float32))
        .astype(jnp.bfloat16)
        .reshape(shape)
    )
    conv_values = conv_result.astype(jnp.float32)
    local_moments = jnp.stack(
        (jnp.sum(conv_values, axis=1), jnp.sum(conv_values * conv_values, axis=1))
    )
    own_kernels = lax.axis_size("tp") == 4 and gate_weight.shape[0] == 1
    if own_kernels:
        full_rows, full_cot, all_moments = dispatch(sent_rows, sent_cot, local_moments, sp_count)
        full_rows = full_rows.reshape(1, experts * capacity, -1)
        full_cot = full_cot.reshape(1, experts * capacity, -1)
        moments = jnp.sum(all_moments, axis=0)
    else:
        got_rows, got_cot = (
            lax.all_to_all(sent_rows, "sp", split_axis=0, concat_axis=1, tiled=True),
            lax.all_to_all(sent_cot, "sp", split_axis=0, concat_axis=1, tiled=True),
        )
        full_rows, full_cot = (
            lax.all_gather(got_rows, "tp", axis=2, tiled=True),
            lax.all_gather(got_cot, "tp", axis=2, tiled=True),
        )
        moments = lax.psum(local_moments, "tp")
    grad_gate, grad_up, grad_down, partial_value = expert_backward(
        full_rows[0], full_cot[0], gate_weight[0], up_weight[0], down_weight[0]
    )
    if own_kernels:
        returned = send_home(partial_value.reshape(experts, capacity, -1), sp_count)
    else:
        summed = lax.psum_scatter(partial_value, "tp", scatter_dimension=2, tiled=True)
        returned = lax.all_to_all(summed, "sp", split_axis=1, concat_axis=0, tiled=True)
    moe_grad = contract_rows(pick, returned.reshape(experts * capacity, -1))
    total_cot = (out_cotangent.astype(jnp.float32) + moe_grad).astype(jnp.bfloat16)
    row_mean = moments[0][:, None] / C
    row_var = moments[1][:, None] / C - row_mean * row_mean
    inv_scale = lax.rsqrt(row_var + NORM_EPS)
    normed = (conv_values - row_mean) * inv_scale
    linear = normed * norm_gain[None, :]
    lin_sigmoid = jax.nn.sigmoid(linear)
    act_out = (linear * lin_sigmoid).astype(jnp.bfloat16)
    cot_full = lax.all_gather(total_cot, "tp", axis=1, tiled=True)
    act_cot = contract_cols(cot_full, proj_weight)
    grad_proj = lax.psum_scatter(
        contract_rows(cot_full, act_out).astype(jnp.bfloat16), "sp", scatter_dimension=0, tiled=True
    ).astype(jnp.float32)
    norm_cot = act_cot * lin_sigmoid * (1.0 + linear * (1.0 - lin_sigmoid)) * norm_gain[None, :]
    cot_sums = lax.psum((jnp.sum(norm_cot, axis=1), jnp.sum(norm_cot * normed, axis=1)), "tp")
    conv_cot = inv_scale * (
        norm_cot - cot_sums[0][:, None] / C - normed * (cot_sums[1][:, None] / C)
    )
    reach_rows = conv_taps.shape[0] - 1
    next_block = from_behind(conv_cot[:reach_rows], "sp", -1)
    extended = jnp.concatenate([conv_cot, next_block], axis=0)
    glu_cot = lax.conv_general_dilated(
        extended[None],
        jnp.flip(conv_taps, 0)[:, None, :],
        (1,),
        "VALID",
        dimension_numbers=("NWC", "WIO", "NWC"),
        feature_group_count=conv_taps.shape[1],
        precision=lax.Precision.HIGHEST,
    )[0]
    gate_sigmoid = jax.nn.sigmoid(glu_gate.astype(jnp.float32))
    grad_value = (glu_cot * gate_sigmoid).astype(jnp.bfloat16)
    grad_glu_gate = (
        glu_cot * glu_value.astype(jnp.float32) * gate_sigmoid * (1.0 - gate_sigmoid)
    ).astype(jnp.bfloat16)
    return (grad_gate, grad_up, grad_down, grad_proj, grad_value, grad_glu_gate)


def solution(mesh):
    in_specs = (
        P("sp", "tp"),
        P("sp", "tp"),
        P("sp", None),
        P("sp", None),
        P("sp", "tp", None),
        P("sp", "tp", None),
        P("sp", "tp", None),
        P("sp", "tp"),
        P("sp", "tp"),
        P("sp", "tp"),
        P(None, "tp"),
        P("tp"),
        P("tp", None),
    )
    out_specs = (
        P("sp", "tp", None),
        P("sp", "tp", None),
        P("sp", "tp", None),
        P("sp", "tp"),
        P("sp", "tp"),
        P("sp", "tp"),
    )
    return jax.shard_map(body, mesh=mesh, in_specs=in_specs, out_specs=out_specs, check_vma=False)
```

profile of v0, /device:TPU:0, one launch (start us, length us, event | category | flops | bytes accessed | tf_op | source)
XLA Modules:
  0.0 239.6 jit_solution(3764930070856537622)
XLA Ops:
  7.2 0.9 copy.55
  8.2 0.1 eq.60
  8.3 0.1 eq.56
  8.5 1.4 reduce-window.6
  9.9 0.1 slice.38
  10.0 0.1 copy.57
  10.1 0.2 reduce-window.9
  10.3 0.1 copy.58
  10.4 0.1 fusion.53
  10.5 0.1 reduce_sum.66
  10.6 0.1 copy.59
  10.7 0.7 multiply_add_fusion
  11.4 0.8 slice_reduce_fusion.3
  12.2 1.1 convert_reduce_fusion
  13.3 2.8 %convolution_convert_fusion.1 = bf16[960,512]{1,0:T(8,128)(2,1)} fusion(bf16[320,512]{1,0:T(8,128)(2,1)} %param.13, s32[320]{0:T(512)S(1)} %get-tuple-element.21, s32[320]{0:T(512)S(1)} %get-tuple-element.20), kind=kOutput, calls=%fused_computation.6 | convolution fusion | flops 315985920 | bytes 1313280 | tf_op jit(solution)/shard_map/dot_general | solution.py:340
  16.1 0.4 add_reduce_fusion
  16.5 1.8 multiply_convert_fusion
  18.3 0.6 pad_maximum_fusion.stats_ref
  18.9 80.7 %shard_map.172 = (bf16[8,120,2048]{2,1,0:T(8,128)(2,1)}, bf16[8,120,2048]{2,1,0:T(8,128)(2,1)}, f32[4,2,320]{2,1,0:T(2,128)}) custom-call(bf16[8,120,512]{2,1,0:T(8,128)(2,1)} %bitcast.67, bf16[8,120,512]{2,1,0:T(8,128)(2,1)} %bitcast.68, f32[2,320]{1,0:T(2,128)} %pad_maximum_fusion.stats_ref), custom_call_target="tpu_custom_call" | custom-call | tf_op jit(solution)/shard_map/pallas_call | solution.py:163
  99.7 3.5 %fusion.6 = f32[960,256]{1,0:T(8,128)S(1)} fusion(bf16[960,2048]{1,0:T(8,128)(2,1)} %bitcast.72, bf16[1,256,2048]{2,1,0:T(8,128)(2,1)S(1)} %copy-done), kind=kOutput, calls=%fused_computation.19 | convolution fusion | flops 1006632960 | bytes 5963776 | tf_op jit(solution)/shard_map/dot_general | solution.py:280
  103.2 0.1 copy-done.7
  103.3 1.2 fusion.9
  104.5 0.9 copy-done.8
  105.4 0.6 copy-done.10
  106.0 1.5 multiply_convert_fusion.2
  107.5 1.2 fusion.4
  108.7 3.3 %add_convert_fusion = bf16[960,2048]{1,0:T(8,128)(2,1)} fusion(f32[960,2048]{1,0:T(8,128)S(1)} %fusion.4, bf16[960,256]{1,0:T(8,128)(2,1)S(1)} %get-tuple-element.24, bf16[1,256,2048]{2,1,0:T(8,128)(2,1)S(1)} %copy-done.1), kind=kOutput, calls=%fused_computation | convolution fusion | flops 1010565120 | bytes 13336576 | tf_op jit(solution)/shard_map/dot_general | solution.py:299
  112.0 53.9 %shard_map.173 = bf16[8,120,512]{2,1,0:T(8,128)(2,1)} custom-call(bf16[8,120,2048]{2,1,0:T(8,128)(2,1)} %bitcast.65), custom_call_target="tpu_custom_call" | custom-call | tf_op jit(solution)/shard_map/pallas_call | solution.py:258
  165.9 2.5 %fusion.1 = bf16[320,512]{1,0:T(8,128)(2,1)} fusion(bf16[960,512]{1,0:T(8,128)(2,1)} %bitcast.66, bf16[320,512]{1,0:T(8,128)(2,1)S(1)} %copy-done.12, s32[320]{0:T(512)S(1)} %get-tuple-element.21, s32[320]{0:T(512)S(1)} %get-tuple-element.20), kind=kOutput, calls=%fused_computation.12 | convolution fusion | flops 315985920 | bytes 1640960 | tf_op jit(solution)/shard_map/dot_general | solution.py:274
  168.4 0.2 reduce-scatter.2.cloned.1.call-start
  168.7 5.1 %convolution_bitcast_fusion = f32[1,256,2048]{2,1,0:T(8,128)} fusion(bf16[960,2048]{1,0:T(8,128)(2,1)} %bitcast.76, f32[960,256]{1,0:T(8,128)} %copy-done.15, f32[960,256]{1,0:T(8,128)S(1)} %fusion.6), kind=kOutput, calls=%fused_computation.1 | convolution fusion | flops 1008107520 | bytes 7995392 | tf_op jit(solution)/shard_map/dot_general | solution.py:274
  173.8 21.3 %all-gather.2.cloned.1.call-done = bf16[320,2048]{1,0:T(8,128)(2,1)} async-done(((bf16[320,512]{1,0:T(8,128)(2,1)}), bf16[320,2048]{1,0:T(8,128)(2,1)}) %all-gather.2.cloned.1.call-update) | async-done | bytes 1310736 | tf_op jit(solution)/shard_map/all_gather | solution.py:386
  195.1 3.2 %convolution_convert_fusion = bf16[2048,256]{1,0:T(8,128)(2,1)} fusion(bf16[320,2048]{1,0:T(8,128)(2,1)} %all-gather.2.cloned.1.call-done, bf16[320,256]{1,0:T(8,128)(2,1)S(1)} %copy-done.2, f32[256]{0:T(256)S(1)} %copy-done.13, f32[320]{0:T(512)S(1)} %add_rsqrt_fusion, f32[320]{0:T(512)S(1)} %get-tuple-element.16), kind=kOutput, calls=%fused_computation.4 | convolution fusion | flops 336805888 | bytes 2526720 | tf_op jit(solution)/shard_map/dot_general | solution.py:274
  198.4 4.9 %convolution_bitcast_fusion.2 = f32[1,256,2048]{2,1,0:T(8,128)} fusion(bf16[960,256]{1,0:T(8,128)(2,1)S(1)} %get-tuple-element.25, bf16[960,2048]{1,0:T(8,128)(2,1)} %bitcast.73), kind=kOutput, calls=%fused_computation.3 | convolution fusion | flops 1006632960 | bytes 6520832 | tf_op jit(solution)/shard_map/dot_general | solution.py:274
  203.2 0.7 fusion.62
  203.9 8.9 %all-reduce = (f32[320]{0:T(512)S(1)}, f32[320]{0:T(512)S(1)}) all-reduce(f32[320]{0:T(512)S(1)} %get-tuple-element.13, f32[320]{0:T(512)S(1)} %get-tuple-element.12), channel_id=1, replica_groups=mesh['sp'=8,'tp'=4] {'tp'}, use_global_device_ids=true, to_apply=%region_11.12 | all-reduce | flops 640 | bytes 5120 | tf_op jit(solution)/shard_map/psum | solution.py:392
  212.8 0.2 fusion.42
  213.1 1.3 collective-permute-start
  214.4 4.7 %convolution_bitcast_fusion.1 = f32[1,256,2048]{2,1,0:T(8,128)} fusion(bf16[960,256]{1,0:T(8,128)(2,1)S(1)} %get-tuple-element.24, bf16[960,2048]{1,0:T(8,128)(2,1)} %bitcast.74), kind=kOutput, calls=%fused_computation.2 | convolution fusion | flops 1006632960 | bytes 6520832 | tf_op jit(solution)/shard_map/dot_general | solution.py:274
  219.1 0.1 rev.4
  219.3 0.4 reshape.86
  219.6 0.1 copy.61
  219.7 0.1 copy-done.14
  219.8 0.8 convolution_select_fusion
  220.6 0.1 copy.63
  220.8 0.8 multiply_convert_fusion.5
  221.7 9.4 %reduce-scatter.2.cloned.1.call-done = bf16[256,256]{1,0:T(8,128)(2,1)} async-done(((bf16[2048,256]{1,0:T(8,128)(2,1)}), bf16[256,256]{1,0:T(8,128)(2,1)}) %reduce-scatter.2.cloned.1.call-update) | async-done | bytes 131088 | tf_op jit(solution)/shard_map/reduce_scatter | solution.py:388
  231.1 1.6 convert_element_type.69
  (45 shorter events, 0.4 us)
Async XLA Ops:
  7.2 92.5 %copy-start = (bf16[1,256,2048]{2,1,0:T(8,128)(2,1)S(1)}, bf16[1,256,2048]{2,1,0:T(8,128)(2,1)}, u32[]{:S(2)}) copy-start(bf16[1,256,2048]{2,1,0:T(8,128)(2,1)} %param.17) | copy-start | bytes 3145732
  7.2 9.3 %copy-start.12 = (bf16[320,512]{1,0:T(8,128)(2,1)S(1)}, bf16[320,512]{1,0:T(8,128)(2,1)}, u32[]{:S(2)}) copy-start(bf16[320,512]{1,0:T(8,128)(2,1)} %param.14) | copy-start | bytes 983044
  7.2 187.9 %all-gather.2.cloned.1.call-start = ((), (), s32[]{:S(2)}) async-start(), calls=%async_computation.1 | async-start | bytes 1638400 | tf_op jit(solution)/shard_map/all_gather | solution.py:386
  99.7 3.5 %copy-start.1 = (bf16[1,256,2048]{2,1,0:T(8,128)(2,1)S(1)}, bf16[1,256,2048]{2,1,0:T(8,128)(2,1)}, u32[]{:S(2)}) copy-start(bf16[1,256,2048]{2,1,0:T(8,128)(2,1)} %param.18) | copy-start | bytes 3145732
  99.7 3.6 %copy-start.7 = (bf16[8,120,2048]{2,1,0:T(8,128)(2,1)S(1)}, bf16[8,120,2048]{2,1,0:T(8,128)(2,1)}, u32[]{:S(2)}) copy-start(bf16[8,120,2048]{2,1,0:T(8,128)(2,1)} %get-tuple-element.10) | copy-start | bytes 11796484
  103.3 2.1 copy-start.8
  103.3 2.8 %copy-start.10 = (bf16[1,256,2048]{2,1,0:T(8,128)(2,1)S(1)}, bf16[1,256,2048]{2,1,0:T(8,128)(2,1)}, u32[]{:S(2)}) copy-start(bf16[1,256,2048]{2,1,0:T(8,128)(2,1)} %param.19) | copy-start | bytes 3145732
  104.5 3.0 %copy-start.15 = (f32[960,256]{1,0:T(8,128)}, f32[960,256]{1,0:T(8,128)S(1)}, u32[]{:S(2)}) copy-start(f32[960,256]{1,0:T(8,128)S(1)} %fusion.9) | copy-start | bytes 2949124
  165.9 2.8 %copy-start.6 = (f32[4,2,320]{2,1,0:T(2,128)S(1)}, f32[4,2,320]{2,1,0:T(2,128)}, u32[]{:S(2)}) copy-start(f32[4,2,320]{2,1,0:T(2,128)} %get-tuple-element.11) | copy-start | bytes 30724
  168.4 62.7 %reduce-scatter.2.cloned.1.call-start = ((), (), s32[]{:S(2)}) async-start(), calls=%async_computation.2 | async-start | bytes 1179648 | tf_op jit(solution)/shard_map/reduce_scatter | solution.py:388
  168.7 26.4 %copy-start.2 = (bf16[320,256]{1,0:T(8,128)(2,1)S(1)}, bf16[320,256]{1,0:T(8,128)(2,1)}, u32[]{:S(2)}) copy-start(bf16[320,256]{1,0:T(8,128)(2,1)} %param.22) | copy-start | bytes 491524
  168.7 26.4 %copy-start.13 = (f32[256]{0:T(256)S(1)}, f32[256]{0:T(256)}, u32[]{:S(2)}) copy-start(f32[256]{0:T(256)} %param.24) | copy-start | bytes 3076
  198.3 4.9 %copy-start.9 = (bf16[320,2048]{1,0:T(8,128)(2,1)S(1)}, bf16[320,2048]{1,0:T(8,128)(2,1)}, u32[]{:S(2)}) copy-start(bf16[320,2048]{1,0:T(8,128)(2,1)} %all-gather.2.cloned.1.call-done) | copy-start | bytes 3932164
  198.3 4.9 %copy-start.11 = (bf16[256,2048]{1,0:T(8,128)(2,1)S(1)}, bf16[256,2048]{1,0:T(8,128)(2,1)}, u32[]{:S(2)}) copy-start(bf16[256,2048]{1,0:T(8,128)(2,1)} %param.25) | copy-start | bytes 3145732
  213.1 6.0 %copy-start.5 = (f32[31,256]{1,0:T(8,128)S(1)}, f32[31,256]{1,0:T(8,128)}, u32[]{:S(2)}) copy-start(f32[31,256]{1,0:T(8,128)} %param.23) | copy-start | bytes 95236
  213.1 6.1 %collective-permute-start = (f32[30,256]{1,0:T(8,128)S(1)}, f32[30,256]{1,0:T(8,128)S(1)}, u32[]{:S(2)}, u32[]{:S(2)}) collective-permute-start(f32[30,256]{1,0:T(8,128)S(1)} %slice.43), channel_id=1, source_target_pairs={{4,0},{8,4},{12,8},{16,12},{20,16},{24,20},{28,24},{5,1},{9,5},{13... | collective-permute-start | bytes 92168 | tf_op jit(solution)/shard_map/ppermute | solution.py:22
  219.1 0.7 copy-start.14
  219.8 0.9 copy-start.3
  219.8 1.0 copy-start.4
Sparse Core Ops, SparseCore 0:
  168.5 26.5 all-gather.1
  198.4 32.6 reduce-scatter.1
where the time goes:
time: 240 us
  Pallas kernels  135 us (56%)
  matrix products  37 us (15%)
  waiting for transfers between devices  30.8 us (13%)
  between operations  14.4 us (6%)
  blocking collectives  8.94 us (4%)
  other arithmetic  7.26 us (3%)
  local copies, waits for them, and re-layouts  5.05 us (2%)
    pallas_call x1, Pallas kernels, dispatch(): pl.pallas_call(functools.partial(dispatch_kernel, n_sp), out_shape=(full,...  80.7 us
    pallas_call x1, Pallas kernels, send_home(): pl.pallas_call(functools.partial(return_kernel, n_sp), out_shape=jax.Shap...  53.9 us
    all_gather x1, waiting for transfers between devices, body(): cot_full = lax.all_gather(total_cot, 'tp', axis=1, tiled=True)  21.3 us
    dot_general x5, matrix products, contract_rows(): lax.dot_general(left, right, (((0,), (0,)), ((), ())), preferred_element_...  20.3 us
    reduce_scatter x1, waiting for transfers between devices, body(): lax.psum_scatter(contract_rows(cot_full, act_out).astype(jnp.bfloat16), '...  9.45 us
    psum x1, blocking collectives, body(): lax.psum((jnp.sum(norm_cot, axis=1), jnp.sum(norm_cot * normed, axis=1)),...  8.94 us
    dot_general x4, matrix products, contract_cols(): lax.dot_general(left, right, (((1,), (1,)), ((), ())), preferred_element_...  6.88 us
  transfers between devices with their start and end apart: 3, of which 2 were waited for; matrix products, arithmetic and copies ran while one was open for 8% of the time, Pallas kernels for 0%

commit v1 on v0

--- a/solution.py
+++ b/solution.py
@@ -118,7 +118,7 @@
         stat_copies.append(copy)
     all_stats[0] = stats_ref[...]
 
-    lag = 1
+    lag = 2
     work = [(which, step) for which in range(2) for step in range(n_sp)]
     hops = {}
     for turn in range(len(work) + lag):
@@ -204,12 +204,17 @@
         return piece(turn, mask)[...].astype(jnp.float32)
 
     crossing, direct, summed, home = {}, {}, {}, {}
-    for turn in range(n_sp):
+
+    def send_out(turn):
         first, second = order(turn)
         crossing[turn] = along_tp(turn, piece(turn, first + second), first, 1)
         crossing[turn].start()
         direct[turn] = along_tp(turn, piece(turn, first), first, 0)
         direct[turn].start()
+
+    ahead = min(2, n_sp)
+    for turn in range(ahead):
+        send_out(turn)
     for turn in range(n_sp + 1):
         if turn < n_sp:
             first, second = order(turn)
@@ -219,6 +224,8 @@
             ).astype(passing.dtype)
             summed[turn] = along_tp(turn, passing.at[turn], second, 2)
             summed[turn].start()
+            if turn + ahead < n_sp:
+                send_out(turn + ahead)
         if turn >= 1:
             last = turn - 1
             direct[last].wait_recv()
@@ -270,6 +277,66 @@
     )(partial)
 
 
+def gather_kernel(block_ref, full_ref, local_sem, send_sem, recv_sem):
+    sp, tp = lax.axis_index("sp"), lax.axis_index("tp")
+    chunks, _, width = block_ref.shape
+    barrier = pltpu.get_barrier_semaphore()
+    for mask in (1, 2):
+        pl.semaphore_signal(barrier, inc=1, device_id=(sp, flip(tp, mask)), device_id_type=MESH)
+    pl.semaphore_wait(barrier, 2)
+
+    def along_tp(chunk, source, origin, hop, slot):
+        return pltpu.make_async_remote_copy(
+            src_ref=source,
+            dst_ref=full_ref.at[chunk, :, columns(flip(tp, origin), width)],
+            send_sem=send_sem.at[chunk, slot],
+            recv_sem=recv_sem.at[chunk, slot],
+            device_id=(sp, flip(tp, hop)),
+            device_id_type=MESH,
+        )
+
+    hops = []
+    for chunk in range(chunks):
+        first, second = (1, 2) if chunk % 2 == 0 else (2, 1)
+        near = along_tp(chunk, block_ref.at[chunk], 0, first, 0)
+        near.start()
+        hops.append([near])
+    own = pltpu.make_async_copy(block_ref, full_ref.at[:, :, columns(tp, width)], local_sem)
+    own.start()
+    for chunk in range(chunks):
+        first, second = (1, 2) if chunk % 2 == 0 else (2, 1)
+        far = along_tp(chunk, block_ref.at[chunk], 0, second, 1)
+        far.start()
+        hops[chunk].append(far)
+    for chunk in range(chunks):
+        first, second = (1, 2) if chunk % 2 == 0 else (2, 1)
+        hops[chunk][0].wait_recv()
+        source = full_ref.at[chunk, :, columns(flip(tp, first), width)]
+        onward = along_tp(chunk, source, first, second, 2)
+        onward.start()
+        hops[chunk].append(onward)
+    own.wait()
+    for near, far, onward in hops:
+        near.wait_send()
+        far.wait()
+        onward.wait()
+
+
+def gather_features(block, chunks):
+    rows, width = block.shape
+    vmem = pl.BlockSpec(memory_space=pltpu.VMEM)
+    dma = pltpu.SemaphoreType.DMA
+    full = pl.pallas_call(
+        gather_kernel,
+        out_shape=jax.ShapeDtypeStruct((chunks, rows // chunks, 4 * width), block.dtype),
+        in_specs=[vmem],
+        out_specs=vmem,
+        scratch_shapes=[dma(()), dma((chunks, 3)), dma((chunks, 3))],
+        compiler_params=pltpu.CompilerParams(collective_id=2, has_side_effects=True),
+    )(block.reshape(chunks, rows // chunks, width))
+    return full.reshape(rows, -1)
+
+
 def contract_rows(left, right):
     return lax.dot_general(
         left, right, (((0,), (0,)), ((), ())), preferred_element_type=jnp.float32
@@ -383,7 +450,10 @@
     linear = normed * norm_gain[None, :]
     lin_sigmoid = jax.nn.sigmoid(linear)
     act_out = (linear * lin_sigmoid).astype(jnp.bfloat16)
-    cot_full = lax.all_gather(total_cot, "tp", axis=1, tiled=True)
+    if own_kernels:
+        cot_full = gather_features(total_cot, 4 if token_count % 32 == 0 else 1)
+    else:
+        cot_full = lax.all_gather(total_cot, "tp", axis=1, tiled=True)
     act_cot = contract_cols(cot_full, proj_weight)
     grad_proj = lax.psum_scatter(
         contract_rows(cot_full, act_out).astype(jnp.bfloat16), "sp", scatter_dimension=0, tiled=True

time: 240 us -> 217 us (0.904)
  waiting for transfers between devices: 30.8 us -> 4.49 us
  Pallas kernels: 135 us -> 139 us
  matrix products: 37 us -> 34.4 us
    all_gather x1 -> x0, waiting for transfers between devices: 21.3 us -> none  [body(): cot_full = lax.all_gather(total_cot, 'tp', axis=1, tiled=True)]
    pallas_call x0 -> x1, Pallas kernels: none -> 14.7 us  [gather_features(): pl.pallas_call(gather_kernel, out_shape=jax.ShapeDtypeStruct((chunks, row...]
    pallas_call x1, Pallas kernels: 53.9 us -> 41.4 us  [send_home(): pl.pallas_call(functools.partial(return_kernel, n_sp), out_shape=jax.Shap...]
    reduce_scatter x1, waiting for transfers between devices: 9.45 us -> 4.47 us  [body(): lax.psum_scatter(contract_rows(cot_full, act_out).astype(jnp.bfloat16), '...]
    dot_general x5, matrix products: 20.3 us -> 15.9 us  [contract_rows(): lax.dot_general(left, right, (((0,), (0,)), ((), ())), preferred_element_...]
  transfers between devices with their start and end apart: 3 -> 2, of which waited for: 2 -> 1; matrix products, arithmetic and copies ran while one was open for 8% -> 7% of each run, Pallas kernels for 0% -> 0%
where the time goes in v1:
time: 217 us; the launch traced here: 216 us
  Pallas kernels  139 us (64%)
  matrix products  34.4 us (16%)
  between operations  14.5 us (7%)
  blocking collectives  8.89 us (4%)
  other arithmetic  8.23 us (4%)
  local copies, waits for them, and re-layouts  5.41 us (2%)
  waiting for transfers between devices  4.49 us (2%)
    pallas_call x1, Pallas kernels, dispatch(): pl.pallas_call(functools.partial(dispatch_kernel, n_sp), out_shape=(full,...  82.8 us
    pallas_call x1, Pallas kernels, send_home(): pl.pallas_call(functools.partial(return_kernel, n_sp), out_shape=jax.Shap...  41.4 us
    dot_general x5, matrix products, contract_rows(): lax.dot_general(left, right, (((0,), (0,)), ((), ())), preferred_element_...  15.9 us
    pallas_call x1, Pallas kernels, gather_features(): pl.pallas_call(gather_kernel, out_shape=jax.ShapeDtypeStruct((chunks, row...  14.7 us
    psum x1, blocking collectives, body(): lax.psum((jnp.sum(norm_cot, axis=1), jnp.sum(norm_cot * normed, axis=1)),...  8.89 us
    dot_general x4, matrix products, contract_cols(): lax.dot_general(left, right, (((1,), (1,)), ((), ())), preferred_element_...  8.7 us
    reduce_scatter x1, waiting for transfers between devices, body(): lax.psum_scatter(contract_rows(cot_full, act_out).astype(jnp.bfloat16), '...  4.47 us
  transfers between devices with their start and end apart: 2, of which 1 were waited for; matrix products, arithmetic and copies ran while one was open for 7% of the time, Pallas kernels for 0%

profile of v1, /device:TPU:0, one launch (start us, length us, event | category | flops | bytes accessed | tf_op | source)
XLA Modules:
  0.0 216.4 jit_solution(435791833485792497)
XLA Ops:
  7.2 0.9 copy.55
  8.2 0.1 eq.60
  8.3 0.1 eq.56
  8.5 1.4 reduce-window.6
  9.9 0.1 slice.38
  10.0 0.1 copy.57
  10.1 0.2 reduce-window.9
  10.3 0.1 copy.58
  10.4 0.1 fusion.53
  10.5 0.1 reduce_sum.66
  10.6 0.1 copy.59
  10.7 0.7 multiply_add_fusion
  11.4 0.8 slice_reduce_fusion.3
  12.2 1.1 convert_reduce_fusion
  13.3 2.8 %convolution_convert_fusion.1 = bf16[960,512]{1,0:T(8,128)(2,1)} fusion(bf16[320,512]{1,0:T(8,128)(2,1)} %param.13, s32[320]{0:T(512)S(1)} %get-tuple-element.21, s32[320]{0:T(512)S(1)} %get-tuple-element.20), kind=kOutput, calls=%fused_computation.6 | convolution fusion | flops 315985920 | bytes 1313280 | tf_op jit(solution)/shard_map/dot_general | solution.py:407
  16.1 0.4 add_reduce_fusion
  16.5 1.8 multiply_convert_fusion
  18.3 0.6 pad_maximum_fusion.stats_ref
  18.9 82.8 %shard_map.172 = (bf16[8,120,2048]{2,1,0:T(8,128)(2,1)}, bf16[8,120,2048]{2,1,0:T(8,128)(2,1)}, f32[4,2,320]{2,1,0:T(2,128)}) custom-call(bf16[8,120,512]{2,1,0:T(8,128)(2,1)} %bitcast.71, bf16[8,120,512]{2,1,0:T(8,128)(2,1)} %bitcast.72, f32[2,320]{1,0:T(2,128)} %pad_maximum_fusion.stats_ref), custom_call_target="tpu_custom_call" | custom-call | tf_op jit(solution)/shard_map/pallas_call | solution.py:163
  101.8 3.5 %fusion.6 = f32[960,256]{1,0:T(8,128)S(1)} fusion(bf16[960,2048]{1,0:T(8,128)(2,1)} %bitcast.77, bf16[1,256,2048]{2,1,0:T(8,128)(2,1)S(1)} %copy-done), kind=kOutput, calls=%fused_computation.19 | convolution fusion | flops 1006632960 | bytes 5963776 | tf_op jit(solution)/shard_map/dot_general | solution.py:347
  105.3 0.1 copy-done.8
  105.4 1.2 fusion.9
  106.7 1.6 copy-done.10
  108.2 0.3 copy-done.12
  108.5 1.5 multiply_convert_fusion.2
  110.0 1.2 fusion.4
  111.2 3.3 %add_convert_fusion = bf16[960,2048]{1,0:T(8,128)(2,1)} fusion(f32[960,2048]{1,0:T(8,128)S(1)} %fusion.4, bf16[960,256]{1,0:T(8,128)(2,1)S(1)} %get-tuple-element.24, bf16[1,256,2048]{2,1,0:T(8,128)(2,1)S(1)} %copy-done.2), kind=kOutput, calls=%fused_computation | convolution fusion | flops 1010565120 | bytes 13336576 | tf_op jit(solution)/shard_map/dot_general | solution.py:366
  114.5 41.4 %shard_map.173 = bf16[8,120,512]{2,1,0:T(8,128)(2,1)} custom-call(bf16[8,120,2048]{2,1,0:T(8,128)(2,1)} %bitcast.67), custom_call_target="tpu_custom_call" | custom-call | tf_op jit(solution)/shard_map/pallas_call | solution.py:265
  155.9 2.5 %fusion.1 = bf16[320,512]{1,0:T(8,128)(2,1)} fusion(bf16[960,512]{1,0:T(8,128)(2,1)} %bitcast.70, bf16[320,512]{1,0:T(8,128)(2,1)S(1)} %copy-done.13, s32[320]{0:T(512)S(1)} %get-tuple-element.21, s32[320]{0:T(512)S(1)} %get-tuple-element.20), kind=kOutput, calls=%fused_computation.12 | convolution fusion | flops 315985920 | bytes 1640960 | tf_op jit(solution)/shard_map/dot_general | solution.py:341
  158.5 14.7 %shard_map.174 = bf16[4,80,2048]{2,1,0:T(8,128)(2,1)} custom-call(bf16[4,80,512]{2,1,0:T(8,128)(2,1)} %bitcast.73), custom_call_target="tpu_custom_call" | custom-call | tf_op jit(solution)/shard_map/pallas_call | solution.py:329
  173.2 3.3 %convolution_convert_fusion = bf16[2048,256]{1,0:T(8,128)(2,1)} fusion(bf16[320,2048]{1,0:T(8,128)(2,1)} %bitcast.68, bf16[320,256]{1,0:T(8,128)(2,1)S(1)} %copy-done.3, f32[256]{0:T(256)S(1)} %copy-done.14, f32[320]{0:T(512)S(1)} %add_rsqrt_fusion, f32[320]{0:T(512)S(1)} %get-tuple-element.16), kind=kOutput, calls=%fused_computation.4 | convolution fusion | flops 336805888 | bytes 2526720 | tf_op jit(solution)/shard_map/dot_general | solution.py:341
  176.5 2.5 %fusion.62 = (f32[320]{0:T(512)S(1)}, f32[320]{0:T(512)S(1)}, f32[320,256]{1,0:T(8,128)}) fusion(f32[320]{0:T(512)S(1)} %add_rsqrt_fusion, f32[320]{0:T(512)S(1)} %get-tuple-element.16, bf16[320,256]{1,0:T(8,128)(2,1)S(1)} %copy-done.3, f32[256]{0:T(256)S(1)} %copy-done.14, bf16[320,2048]{1,0:T(8,128)(2,1)S(1)} %bitcast.69, bf16[256,2048]{1,0:T(8,128)(2,1)} %param.25), kind=kOutput, calls=%fused_computation.97 | convolution fusion | flops 336854400 | bytes 2856960 | tf_op jit(solution)/shard_map/dot_general | solution.py:347
  179.1 8.9 %all-reduce = (f32[320]{0:T(512)S(1)}, f32[320]{0:T(512)S(1)}) all-reduce(f32[320]{0:T(512)S(1)} %get-tuple-element.13, f32[320]{0:T(512)S(1)} %get-tuple-element.12), channel_id=1, replica_groups=mesh['sp'=8,'tp'=4] {'tp'}, use_global_device_ids=true, to_apply=%region_11.12 | all-reduce | flops 640 | bytes 5120 | tf_op jit(solution)/shard_map/psum | solution.py:462
  188.0 1.2 fusion.42
  189.2 1.6 collective-permute-start
  190.8 4.9 %convolution_bitcast_fusion.2 = f32[1,256,2048]{2,1,0:T(8,128)} fusion(bf16[960,256]{1,0:T(8,128)(2,1)S(1)} %get-tuple-element.25, bf16[960,2048]{1,0:T(8,128)(2,1)} %bitcast.78), kind=kOutput, calls=%fused_computation.3 | convolution fusion | flops 1006632960 | bytes 6520832 | tf_op jit(solution)/shard_map/dot_general | solution.py:341
  195.7 2.7 %convolution_bitcast_fusion = f32[1,256,2048]{2,1,0:T(8,128)} fusion(bf16[960,2048]{1,0:T(8,128)(2,1)S(1)} %bitcast.82, f32[960,256]{1,0:T(8,128)S(1)} %copy-done.19, f32[960,256]{1,0:T(8,128)S(1)} %copy-done.17), kind=kOutput, calls=%fused_computation.1 | convolution fusion | flops 1008107520 | bytes 7995392 | tf_op jit(solution)/shard_map/dot_general | solution.py:341
  198.3 2.6 %convolution_bitcast_fusion.1 = f32[1,256,2048]{2,1,0:T(8,128)} fusion(bf16[960,256]{1,0:T(8,128)(2,1)S(1)} %get-tuple-element.24, bf16[960,2048]{1,0:T(8,128)(2,1)S(1)} %bitcast.80), kind=kOutput, calls=%fused_computation.2 | convolution fusion | flops 1006632960 | bytes 6520832 | tf_op jit(solution)/shard_map/dot_general | solution.py:341
  200.9 0.1 rev.4
  201.1 0.4 reshape.94
  201.5 0.1 copy.61
  201.6 0.1 copy-done.15
  201.6 0.8 convolution_select_fusion
  202.4 0.1 copy.63
  202.6 0.0 copy-done.5
  202.6 0.8 multiply_convert_fusion.5
  203.5 4.5 %reduce-scatter.2.cloned.1.call-done = bf16[256,256]{1,0:T(8,128)(2,1)} async-done(((bf16[2048,256]{1,0:T(8,128)(2,1)}), bf16[256,256]{1,0:T(8,128)(2,1)}) %reduce-scatter.2.cloned.1.call-update) | async-done | bytes 131088 | tf_op jit(solution)/shard_map/reduce_scatter | solution.py:458
  208.0 1.6 convert_element_type.69
  (51 shorter events, 0.4 us)
Async XLA Ops:
  7.2 94.6 %copy-start = (bf16[1,256,2048]{2,1,0:T(8,128)(2,1)S(1)}, bf16[1,256,2048]{2,1,0:T(8,128)(2,1)}, u32[]{:S(2)}) copy-start(bf16[1,256,2048]{2,1,0:T(8,128)(2,1)} %param.17) | copy-start | bytes 3145732
  7.2 9.3 %copy-start.13 = (bf16[320,512]{1,0:T(8,128)(2,1)S(1)}, bf16[320,512]{1,0:T(8,128)(2,1)}, u32[]{:S(2)}) copy-start(bf16[320,512]{1,0:T(8,128)(2,1)} %param.14) | copy-start | bytes 983044
  7.2 200.8 %reduce-scatter.2.cloned.1.call-start = ((), (), s32[]{:S(2)}) async-start(), calls=%async_computation.1 | async-start | bytes 1179648 | tf_op jit(solution)/shard_map/reduce_scatter | solution.py:458
  101.8 3.5 %copy-start.2 = (bf16[1,256,2048]{2,1,0:T(8,128)(2,1)S(1)}, bf16[1,256,2048]{2,1,0:T(8,128)(2,1)}, u32[]{:S(2)}) copy-start(bf16[1,256,2048]{2,1,0:T(8,128)(2,1)} %param.18) | copy-start | bytes 3145732
  101.8 3.6 %copy-start.8 = (bf16[8,120,2048]{2,1,0:T(8,128)(2,1)S(1)}, bf16[8,120,2048]{2,1,0:T(8,128)(2,1)}, u32[]{:S(2)}) copy-start(bf16[8,120,2048]{2,1,0:T(8,128)(2,1)} %get-tuple-element.10) | copy-start | bytes 11796484
  105.4 1.3 copy-start.16
  105.4 2.8 %copy-start.10 = (bf16[8,120,2048]{2,1,0:T(8,128)(2,1)S(1)}, bf16[8,120,2048]{2,1,0:T(8,128)(2,1)}, u32[]{:S(2)}) copy-start(bf16[8,120,2048]{2,1,0:T(8,128)(2,1)} %get-tuple-element.9) | copy-start | bytes 11796484
  105.4 3.1 %copy-start.12 = (bf16[1,256,2048]{2,1,0:T(8,128)(2,1)S(1)}, bf16[1,256,2048]{2,1,0:T(8,128)(2,1)}, u32[]{:S(2)}) copy-start(bf16[1,256,2048]{2,1,0:T(8,128)(2,1)} %param.19) | copy-start | bytes 3145732
  106.6 3.4 %copy-start.18 = (f32[960,256]{1,0:T(8,128)}, f32[960,256]{1,0:T(8,128)S(1)}, u32[]{:S(2)}) copy-start(f32[960,256]{1,0:T(8,128)S(1)} %fusion.9) | copy-start | bytes 2949124
  155.9 17.2 %copy-start.7 = (f32[4,2,320]{2,1,0:T(2,128)S(1)}, f32[4,2,320]{2,1,0:T(2,128)}, u32[]{:S(2)}) copy-start(f32[4,2,320]{2,1,0:T(2,128)} %get-tuple-element.11) | copy-start | bytes 30724
  155.9 17.3 %copy-start.3 = (bf16[320,256]{1,0:T(8,128)(2,1)S(1)}, bf16[320,256]{1,0:T(8,128)(2,1)}, u32[]{:S(2)}) copy-start(bf16[320,256]{1,0:T(8,128)(2,1)} %param.22) | copy-start | bytes 491524
  155.9 17.3 %copy-start.14 = (f32[256]{0:T(256)S(1)}, f32[256]{0:T(256)}, u32[]{:S(2)}) copy-start(f32[256]{0:T(256)} %param.24) | copy-start | bytes 3076
  173.2 3.3 %copy-start.1 = (bf16[4,80,2048]{2,1,0:T(8,128)(2,1)S(1)}, bf16[4,80,2048]{2,1,0:T(8,128)(2,1)}, u32[]{:S(2)}) copy-start(bf16[4,80,2048]{2,1,0:T(8,128)(2,1)} %shard_map.174) | copy-start | bytes 3932164
  189.2 6.5 %copy-start.11 = (bf16[8,120,2048]{2,1,0:T(8,128)(2,1)S(1)}, bf16[8,120,2048]{2,1,0:T(8,128)(2,1)}, u32[]{:S(2)}) copy-start(bf16[8,120,2048]{2,1,0:T(8,128)(2,1)} %get-tuple-element.9) | copy-start | bytes 11796484
  189.2 6.5 %copy-start.17 = (f32[960,256]{1,0:T(8,128)S(1)}, f32[960,256]{1,0:T(8,128)}, u32[]{:S(2)}) copy-start(f32[960,256]{1,0:T(8,128)} %copy-done.16) | copy-start | bytes 2949124
  189.2 6.5 %copy-start.19 = (f32[960,256]{1,0:T(8,128)S(1)}, f32[960,256]{1,0:T(8,128)}, u32[]{:S(2)}) copy-start(f32[960,256]{1,0:T(8,128)} %copy-done.18) | copy-start | bytes 2949124
  189.2 11.8 %collective-permute-start = (f32[30,256]{1,0:T(8,128)S(1)}, f32[30,256]{1,0:T(8,128)S(1)}, u32[]{:S(2)}, u32[]{:S(2)}) collective-permute-start(f32[30,256]{1,0:T(8,128)S(1)} %slice.43), channel_id=1, source_target_pairs={{4,0},{8,4},{12,8},{16,12},{20,16},{24,20},{28,24},{5,1},{9,5},{13... | collective-permute-start | bytes 92168 | tf_op jit(solution)/shard_map/ppermute | solution.py:22
  195.7 2.7 %copy-start.9 = (bf16[8,120,2048]{2,1,0:T(8,128)(2,1)S(1)}, bf16[8,120,2048]{2,1,0:T(8,128)(2,1)}, u32[]{:S(2)}) copy-start(bf16[8,120,2048]{2,1,0:T(8,128)(2,1)} %get-tuple-element.10) | copy-start | bytes 11796484
  198.3 2.6 %copy-start.6 = (f32[31,256]{1,0:T(8,128)S(1)}, f32[31,256]{1,0:T(8,128)}, u32[]{:S(2)}) copy-start(f32[31,256]{1,0:T(8,128)} %param.23) | copy-start | bytes 95236
  200.9 0.7 copy-start.15
  201.6 0.9 copy-start.4
  201.6 1.0 copy-start.5
Sparse Core Ops, SparseCore 0:
  176.6 31.2 reduce-scatter.1
